TPU v7x, 128 devices: a whole 4x4x4 slice. The times are simulated.
128 devices in a mesh: ra: 16 (over z, x), cb: 8 (over y, core).
Axes of the slice: x: 4, y: 4, z: 4, core: 2. Of those that a mesh axis runs over, the one named last changes fastest.
Arguments:
- inputs: bfloat16 [1536, 4096], P(None, 'ra'), may hold values from -12 to 12
- gate_weight: bfloat16 [2, 4096, 11264], P(None, 'ra', 'cb'), may hold values from -0.09375 to 0.09375
- up_weight: bfloat16 [2, 4096, 11264], P(None, 'ra', 'cb'), may hold values from -0.09375 to 0.09375
- down_weight: bfloat16 [2, 11264, 4096], P(None, 'cb', 'ra'), may hold values from -0.0546875 to 0.0546875
- norm_gain: float32 [2, 4096], P(None, 'ra'), may hold values from 0.05 to 8
- norm_shift: float32 [2, 4096], P(None, 'ra'), may hold values from -1.5 to 1.5
Outputs:
- outputs: bfloat16 [1536, 4096], P(None, 'ra')
All inputs are finite; a program needn't handle non-finite values.
Results may differ from a plain program's by a relative error of at most 0.04.
Values may be sent and summed in bfloat16 or wider, within the bound.
No kernel may reach another device: no remote copies, remote signals or barrier semaphores. Data moves between devices by JAX's collectives and lax.ppermute only.
A program may use at most 64 MiB of HBM per device.

v0:
```python
import jax
import jax.numpy as jnp
from jax import lax
from jax.sharding import Mesh
from jax.sharding import PartitionSpec as P

RESIDUAL = 0.5
EPSILON = 1e-05
BF16 = jnp.bfloat16
F32 = jnp.float32


def exchange(parts, axes):
    return lax.all_to_all(parts, axes, 0, 0, tiled=True)


def share(block, axes, peers):
    return exchange(jnp.broadcast_to(block[None], (peers, *block.shape)), axes)


def swap_core(block):
    return lax.ppermute(block, "c", [(0, 1), (1, 0)])


def dot_nt(a, b):
    return lax.dot_general(a, b, (((1,), (1,)), ((), ())), preferred_element_type=F32)


def regroup_weights(gate, up, down):
    stacked = jnp.stack((gate.T, up.T, down))
    rows = stacked.shape[1] // 4
    parts = stacked.reshape(3, 4, rows, 256).transpose(1, 0, 2, 3)
    mine = exchange(parts, "x")
    mine = mine.transpose(1, 2, 0, 3).reshape(3, rows, 1024)
    other = swap_core(mine)
    both = jnp.concatenate((mine, other), axis=1)
    return (both[:2].reshape(2 * 2 * rows, 1024), both[2])


def normed(mixed, row_sum, row_squares, gain, shift):
    mean = row_sum / 4096.0
    var = row_squares / 4096.0 - mean * mean
    out = (mixed - mean[:, None]) * lax.rsqrt(var + EPSILON)[:, None]
    return (out * gain + shift).astype(BF16)


def hidden_units(stream, w_gu):
    partial = dot_nt(stream, w_gu).astype(BF16)
    cols = partial.shape[1] // 2
    summed = exchange(partial.reshape(4, -1, 2 * cols), "z").astype(F32).sum(axis=0)
    hidden = (jax.nn.silu(summed[:, :cols]) * summed[:, cols:]).astype(BF16)
    return share(hidden, "z", 4).reshape(-1, cols)


def per_device(inputs, gate_weight, up_weight, down_weight, norm_gain, norm_shift):
    c = lax.axis_index("c")
    x = lax.axis_index("x")
    y = lax.axis_index("y")
    half = inputs.shape[0] // 2
    quarter = half // 4
    mine = lax.dynamic_slice_in_dim(inputs, c * half + y * quarter, quarter, 0)
    rows = share(mine, "x", 4).transpose(1, 0, 2).reshape(quarter, 1024)
    stream = share(rows, "y", 4).reshape(half, 1024)
    affine = jnp.stack((norm_gain[0], norm_shift[0]))
    affine = lax.all_gather(affine, "x", axis=1, tiled=True)
    gu0, down0 = regroup_weights(gate_weight[0], up_weight[0], down_weight[0])
    gu1, down1 = regroup_weights(gate_weight[1], up_weight[1], down_weight[1])
    hidden = hidden_units(stream, gu0)
    partial = jnp.dot(hidden, down0, preferred_element_type=F32).astype(BF16)
    block = half // 16
    branch = exchange(partial.reshape(16, block, 1024), ("x", "y")).astype(F32).sum(axis=0)
    own = lax.dynamic_slice_in_dim(stream, (x * 4 + y) * block, block, 0)
    mixed = RESIDUAL * own.astype(F32) + branch
    stats = lax.psum(jnp.stack((mixed.sum(axis=1), (mixed * mixed).sum(axis=1))), "z")
    out = normed(mixed, stats[0], stats[1], affine[0], affine[1])
    stream = share(out, ("x", "y"), 16).reshape(half, 1024)
    hidden = hidden_units(stream, gu1)
    partial = jnp.dot(hidden, down1, preferred_element_type=F32).astype(BF16)
    parts = partial.reshape(4, quarter, 4, 256).transpose(2, 0, 1, 3).reshape(16, quarter, 256)
    branch = exchange(parts, ("x", "y")).astype(F32).sum(axis=0)
    own = lax.dynamic_slice(stream, (y * quarter, x * 256), (quarter, 256))
    mixed = RESIDUAL * own.astype(F32) + branch
    stats = lax.psum(jnp.stack((mixed.sum(axis=1), (mixed * mixed).sum(axis=1))), ("z", "x"))
    out = normed(mixed, stats[0], stats[1], norm_gain[1], norm_shift[1])
    ours = share(out, "y", 4).reshape(half, 256)
    theirs = swap_core(ours)
    result = jnp.concatenate((ours, theirs), axis=0)
    swapped = jnp.concatenate((theirs, ours), axis=0)
    return jnp.where(c == 0, result, swapped)


def solution(mesh):
    finer = Mesh(mesh.devices.reshape(4, 4, 4, 2), ("z", "x", "y", "c"))
    ra, cb = (("z", "x"), ("y", "c"))
    in_specs = (
        P(None, ra),
        P(None, ra, cb),
        P(None, ra, cb),
        P(None, cb, ra),
        P(None, ra),
        P(None, ra),
    )
    return jax.shard_map(
        per_device, mesh=finer, in_specs=in_specs, out_specs=P(None, ra), check_vma=False
    )
```

profile of v0, /device:TPU:1, one launch (start us, length us, event | category | flops | bytes accessed | tf_op | source)
XLA Modules:
  0.0 365.9 jit_solution(2115882943331297913)
XLA Ops:
  0.0 2.4 fusion.6
  2.7 2.3 fusion.7
  5.2 2.3 fusion.8
  7.9 30.5 %all_to_all.60 = bf16[4,3,352,256]{3,2,1,0:T(8,128)(2,1)S(1)} all-to-all(bf16[4,3,352,256]{3,2,1,0:T(8,128)(2,1)S(1)} %copy.30), channel_id=1, replica_groups=mesh['z'=4,'x'=4,'y'=4,'c'=2] {'x'}, dimensions={0} | all-to-all | bytes 4325376 | tf_op jit(solution)/shard_map/all_to_all | solution.py:14
  38.7 2.2 collective-permute-start
  41.0 10.2 %all_to_all.61 = bf16[4,192,256]{2,1,0:T(8,128)(2,1)S(1)} all-to-all(bf16[4,192,256]{2,1,0:T(8,128)(2,1)S(1)} %broadcast_in_dim.14), channel_id=1, replica_groups=mesh['z'=4,'x'=4,'y'=4,'c'=2] {'x'}, dimensions={0} | all-to-all | bytes 786432 | tf_op jit(solution)/shard_map/all_to_all | solution.py:14
  52.7 4.4 %all-to-all-start.1 = ((bf16[4,192,1024]{2,1,0:T(8,128)(2,1)}), bf16[4,192,1024]{2,1,0:T(8,128)(2,1)}, u32[]{:S(2)}, u32[]{:S(2)}) async-start(bf16[4,192,1024]{2,1,0:T(8,128)(2,1)} %broadcast_in_dim.16), calls=%async_computation.1 | async-start | bytes 3145728 | tf_op jit(solution)/shard_map/all_to_all | solution.py:14
  59.0 2.0 copy-done.2
  62.9 13.6 %all-to-all-done.1 = bf16[4,192,1024]{2,1,0:T(8,128)(2,1)} async-done(((bf16[4,192,1024]{2,1,0:T(8,128)(2,1)}), bf16[4,192,1024]{2,1,0:T(8,128)(2,1)}, u32[]{:S(2)}, u32[]{:S(2)}) %all-to-all-start.1) | async-done | bytes 1572896 | tf_op jit(solution)/shard_map/all_to_all | solution.py:14
  76.5 4.9 %convolution_convert_fusion.1 = bf16[768,1408]{1,0:T(8,128)(2,1)S(1)} fusion(bf16[768,1024]{1,0:T(8,128)(2,1)} %bitcast.1, bf16[1408,1024]{1,0:T(8,128)(2,1)} %bitcast.85), kind=kOutput, calls=%fused_computation.3 | convolution fusion | flops 2215673856 | bytes 6619136 | tf_op jit(solution)/shard_map/dot_general | solution.py:26
  81.5 29.2 %all_to_all.62 = bf16[4,192,1408]{2,1,0:T(8,128)(2,1)S(1)} all-to-all(bf16[4,192,1408]{2,1,0:T(8,128)(2,1)S(1)} %bitcast.93), channel_id=1, replica_groups=mesh['z'=4,'x'=4,'y'=4,'c'=2] {'z'}, dimensions={0} | all-to-all | bytes 4325376 | tf_op jit(solution)/shard_map/all_to_all | solution.py:14
  112.4 4.4 %all-to-all-start.4 = ((bf16[4,192,704]{2,1,0:T(8,128)(2,1)}), bf16[4,192,704]{2,1,0:T(8,128)(2,1)}, u32[]{:S(2)}, u32[]{:S(2)}) async-start(bf16[4,192,704]{2,1,0:T(8,128)(2,1)} %broadcast_in_dim.17), calls=%async_computation.4 | async-start | bytes 2359296 | tf_op jit(solution)/shard_map/all_to_all | solution.py:14
  119.1 10.4 %all-to-all-done.4 = bf16[4,192,704]{2,1,0:T(8,128)(2,1)} async-done(((bf16[4,192,704]{2,1,0:T(8,128)(2,1)}), bf16[4,192,704]{2,1,0:T(8,128)(2,1)}, u32[]{:S(2)}, u32[]{:S(2)}) %all-to-all-start.4) | async-done | bytes 1081376 | tf_op jit(solution)/shard_map/all_to_all | solution.py:14
  129.5 3.6 all-to-all-start.7
  133.2 4.3 %convolution_convert_fusion.3 = bf16[768,1024]{1,0:T(8,128)(2,1)} fusion(bf16[768,704]{1,0:T(8,128)(2,1)} %bitcast.13, bf16[3,704,1024]{2,1,0:T(8,128)(2,1)} %copy-done.2), kind=kOutput, calls=%fused_computation.9 | convolution fusion | flops 1108082688 | bytes 4194304 | tf_op jit(solution)/shard_map/dot_general | solution.py:69
  137.5 18.0 %all-to-all-done.7 = bf16[4,3,352,256]{3,2,1,0:T(8,128)(2,1)S(1)} async-done(((bf16[4,3,352,256]{3,2,1,0:T(8,128)(2,1)}), bf16[4,3,352,256]{3,2,1,0:T(8,128)(2,1)S(1)}, u32[]{:S(2)}, u32[]{:S(2)}) %all-to-all-start.7) | async-done | bytes 2162720 | tf_op jit(solution)/shard_map/all_to_all | solution.py:14
  155.5 4.4 %all-to-all-start.5 = ((bf16[16,48,1024]{2,1,0:T(8,128)(2,1)}), bf16[16,48,1024]{2,1,0:T(8,128)(2,1)}, u32[]{:S(2)}, u32[]{:S(2)}) async-start(bf16[16,48,1024]{2,1,0:T(8,128)(2,1)} %bitcast.95), calls=%async_computation.5 | async-start | bytes 3145728 | tf_op jit(solution)/shard_map/all_to_all | solution.py:14
  160.0 18.8 %all_gather.3 = f32[2,1024]{1,0:T(2,128)S(1)} all-gather(f32[2,256]{1,0:T(2,128)S(1)} %pad_maximum_fusion), channel_id=1, replica_groups=mesh['z'=4,'x'=4,'y'=4,'c'=2] {'x'}, dimensions={1}, use_global_device_ids=true | all-gather | bytes 10240 | tf_op jit(solution)/shard_map/all_gather | solution.py:65
  180.4 8.3 %collective-permute-start.1 = (bf16[3,352,1024]{2,1,0:T(8,128)(2,1)}, bf16[3,352,1024]{2,1,0:T(8,128)(2,1)S(1)}, u32[]{:S(2)}, u32[]{:S(2)}) collective-permute-start(bf16[3,352,1024]{2,1,0:T(8,128)(2,1)} %bitcast.59), channel_id=1, source_target_pairs={{0,1},{1,0},{2,3},{3,2},{4,5},{5,4},{6,7},{7,6},{8,9},{9,8},{10,11... | collective-permute-start | bytes 6488072 | tf_op jit(solution)/shard_map/ppermute | solution.py:22
  191.5 6.9 %psum.14 = f32[2,48]{1,0:T(2,128)S(1)} all-reduce(f32[2,48]{1,0:T(2,128)S(1)} %pad_maximum_fusion.2), channel_id=1, replica_groups=mesh['z'=4,'x'=4,'y'=4,'c'=2] {'z'}, use_global_device_ids=true, to_apply=%region_4.5 | all-reduce | flops 96 | bytes 768 | tf_op jit(solution)/shard_map/psum | solution.py:74
  200.8 5.1 %all-to-all-start.6 = ((bf16[16,48,1024]{2,1,0:T(8,128)(2,1)}), bf16[16,48,1024]{2,1,0:T(8,128)(2,1)}, u32[]{:S(2)}, u32[]{:S(2)}) async-start(bf16[16,48,1024]{2,1,0:T(8,128)(2,1)} %broadcast_in_dim.18), calls=%async_computation.6 | async-start | bytes 3145728 | tf_op jit(solution)/shard_map/all_to_all | solution.py:14
  211.8 14.5 %all-to-all-done.6 = bf16[16,48,1024]{2,1,0:T(8,128)(2,1)} async-done(((bf16[16,48,1024]{2,1,0:T(8,128)(2,1)}), bf16[16,48,1024]{2,1,0:T(8,128)(2,1)}, u32[]{:S(2)}, u32[]{:S(2)}) %all-to-all-start.6) | async-done | bytes 1572896 | tf_op jit(solution)/shard_map/all_to_all | solution.py:14
  226.3 4.9 %convolution_convert_fusion = bf16[768,1408]{1,0:T(8,128)(2,1)S(1)} fusion(bf16[768,1024]{1,0:T(8,128)(2,1)} %bitcast.22, bf16[1408,1024]{1,0:T(8,128)(2,1)} %bitcast.86), kind=kOutput, calls=%fused_computation.2 | convolution fusion | flops 2215673856 | bytes 6619136 | tf_op jit(solution)/shard_map/dot_general | solution.py:26
  231.3 25.4 %all_to_all.63 = bf16[4,192,1408]{2,1,0:T(8,128)(2,1)S(1)} all-to-all(bf16[4,192,1408]{2,1,0:T(8,128)(2,1)S(1)} %bitcast.94), channel_id=1, replica_groups=mesh['z'=4,'x'=4,'y'=4,'c'=2] {'z'}, dimensions={0} | all-to-all | bytes 4325376 | tf_op jit(solution)/shard_map/all_to_all | solution.py:14
  257.4 13.7 %all_to_all.64 = bf16[4,192,704]{2,1,0:T(8,128)(2,1)S(1)} all-to-all(bf16[4,192,704]{2,1,0:T(8,128)(2,1)S(1)} %broadcast_in_dim.19), channel_id=1, replica_groups=mesh['z'=4,'x'=4,'y'=4,'c'=2] {'z'}, dimensions={0} | all-to-all | bytes 2162688 | tf_op jit(solution)/shard_map/all_to_all | solution.py:14
  271.1 3.9 %convolution_convert_fusion.2 = bf16[768,1024]{1,0:T(8,128)(2,1)} fusion(bf16[768,704]{1,0:T(8,128)(2,1)S(1)} %bitcast.100, bf16[3,704,1024]{2,1,0:T(8,128)(2,1)} %copy-done.3), kind=kOutput, calls=%fused_computation.8 | convolution fusion | flops 1108082688 | bytes 4096000 | tf_op jit(solution)/shard_map/dot_general | solution.py:78
  275.0 2.9 reshape.113
  279.3 10.2 %all-to-all-start.10 = ((bf16[16,192,256]{2,1,0:T(8,128)(2,1)}), bf16[16,192,256]{2,1,0:T(8,128)(2,1)S(1)}, u32[]{:S(2)}, u32[]{:S(2)}) async-start(bf16[16,192,256]{2,1,0:T(8,128)(2,1)} %bitcast.84), calls=%async_computation.10 | async-start | bytes 3145728 | tf_op jit(solution)/shard_map/all_to_all | solution.py:14
  289.6 19.0 %all-to-all-done.10 = bf16[16,192,256]{2,1,0:T(8,128)(2,1)S(1)} async-done(((bf16[16,192,256]{2,1,0:T(8,128)(2,1)}), bf16[16,192,256]{2,1,0:T(8,128)(2,1)S(1)}, u32[]{:S(2)}, u32[]{:S(2)}) %all-to-all-start.10) | async-done | bytes 1572896 | tf_op jit(solution)/shard_map/all_to_all | solution.py:14
  309.9 31.9 %psum.15 = f32[2,192]{1,0:T(2,128)S(1)} all-reduce(f32[2,192]{1,0:T(2,128)S(1)} %pad_maximum_fusion.1), channel_id=1, replica_groups=mesh['z'=4,'x'=4,'y'=4,'c'=2] {'z','x'}, use_global_device_ids=true, to_apply=%region_9.10 | all-reduce | flops 384 | bytes 3072 | tf_op jit(solution)/shard_map/psum | solution.py:83
  342.9 10.1 %all_to_all.65 = bf16[4,192,256]{2,1,0:T(8,128)(2,1)S(1)} all-to-all(bf16[4,192,256]{2,1,0:T(8,128)(2,1)S(1)} %broadcast_in_dim.20), channel_id=1, replica_groups=mesh['z'=4,'x'=4,'y'=4,'c'=2] {'y'}, dimensions={0} | all-to-all | bytes 786432 | tf_op jit(solution)/shard_map/all_to_all | solution.py:14
  353.0 10.3 %collective-permute-start.2 = (bf16[768,256]{1,0:T(8,128)(2,1)S(1)}, bf16[768,256]{1,0:T(8,128)(2,1)S(1)}, u32[]{:S(2)}, u32[]{:S(2)}) collective-permute-start(bf16[768,256]{1,0:T(8,128)(2,1)S(1)} %bitcast.97), channel_id=1, source_target_pairs={{0,1},{1,0},{2,3},{3,2},{4,5},{5,4},{6,7},{7,6},{8,9},{9,8},{10,11... | collective-permute-start | bytes 1179656 | tf_op jit(solution)/shard_map/ppermute | solution.py:22
  (66 shorter events, 30.2 us)
Async XLA Ops:
  0.0 40.9 %copy-start = (bf16[1536,256]{1,0:T(8,128)(2,1)S(1)}, bf16[1536,256]{1,0:T(8,128)(2,1)}, u32[]{:S(2)}) copy-start(bf16[1536,256]{1,0:T(8,128)(2,1)} %param.6) | copy-start | bytes 2359300
  38.7 18.5 %collective-permute-start = (bf16[3,352,1024]{2,1,0:T(8,128)(2,1)S(1)}, bf16[3,352,1024]{2,1,0:T(8,128)(2,1)}, u32[]{:S(2)}, u32[]{:S(2)}) collective-permute-start(bf16[3,352,1024]{2,1,0:T(8,128)(2,1)S(1)} %bitcast.81), channel_id=1, source_target_pairs={{0,1},{1,0},{2,3},{3,2},{4,5},{5,4},{6,7},{7,6},{8,9},{9,8},{10,11... | collective-permute-start | bytes 6488072 | tf_op jit(solution)/shard_map/ppermute | solution.py:22
  52.7 23.9 %all-to-all-start.1 = ((bf16[4,192,1024]{2,1,0:T(8,128)(2,1)}), bf16[4,192,1024]{2,1,0:T(8,128)(2,1)}, u32[]{:S(2)}, u32[]{:S(2)}) async-start(bf16[4,192,1024]{2,1,0:T(8,128)(2,1)} %broadcast_in_dim.16), calls=%async_computation.1 | async-start | bytes 3145728 | tf_op jit(solution)/shard_map/all_to_all | solution.py:14
  59.0 2.1 copy-start.2
  111.2 5.6 %copy-start.4 = (bf16[1,256,1408]{2,1,0:T(8,128)(2,1)S(1)}, bf16[1,256,1408]{2,1,0:T(8,128)(2,1)}, u32[]{:S(2)}) copy-start(bf16[1,256,1408]{2,1,0:T(8,128)(2,1)} %get-tuple-element.9) | copy-start | bytes 2162692
  112.4 4.7 %copy-start.5 = (bf16[1,256,1408]{2,1,0:T(8,128)(2,1)S(1)}, bf16[1,256,1408]{2,1,0:T(8,128)(2,1)}, u32[]{:S(2)}) copy-start(bf16[1,256,1408]{2,1,0:T(8,128)(2,1)} %get-tuple-element.11) | copy-start | bytes 2162692
  112.4 5.0 %copy-start.6 = (bf16[1,1408,256]{2,1,0:T(8,128)(2,1)S(1)}, bf16[1,1408,256]{2,1,0:T(8,128)(2,1)}, u32[]{:S(2)}) copy-start(bf16[1,1408,256]{2,1,0:T(8,128)(2,1)} %get-tuple-element.13) | copy-start | bytes 2162692
  112.4 17.1 %all-to-all-start.4 = ((bf16[4,192,704]{2,1,0:T(8,128)(2,1)}), bf16[4,192,704]{2,1,0:T(8,128)(2,1)}, u32[]{:S(2)}, u32[]{:S(2)}) async-start(bf16[4,192,704]{2,1,0:T(8,128)(2,1)} %broadcast_in_dim.17), calls=%async_computation.4 | async-start | bytes 2359296 | tf_op jit(solution)/shard_map/all_to_all | solution.py:14
  129.5 25.9 %all-to-all-start.7 = ((bf16[4,3,352,256]{3,2,1,0:T(8,128)(2,1)}), bf16[4,3,352,256]{3,2,1,0:T(8,128)(2,1)S(1)}, u32[]{:S(2)}, u32[]{:S(2)}) async-start(bf16[4,3,352,256]{3,2,1,0:T(8,128)(2,1)} %copy.34), calls=%async_computation.7 | async-start | bytes 4325376 | tf_op jit(solution)/shard_map/all_to_all | solution.py:14
  137.5 22.4 %copy-start.7 = (f32[2,256]{1,0:T(2,128)S(1)}, f32[2,256]{1,0:T(2,128)}, u32[]{:S(2)}) copy-start(f32[2,256]{1,0:T(2,128)} %param.10) | copy-start | bytes 6148
  137.5 22.5 %copy-start.8 = (f32[2,256]{1,0:T(2,128)S(1)}, f32[2,256]{1,0:T(2,128)}, u32[]{:S(2)}) copy-start(f32[2,256]{1,0:T(2,128)} %param.11) | copy-start | bytes 6148
  155.5 33.3 %all-to-all-start.5 = ((bf16[16,48,1024]{2,1,0:T(8,128)(2,1)}), bf16[16,48,1024]{2,1,0:T(8,128)(2,1)}, u32[]{:S(2)}, u32[]{:S(2)}) async-start(bf16[16,48,1024]{2,1,0:T(8,128)(2,1)} %bitcast.95), calls=%async_computation.5 | async-start | bytes 3145728 | tf_op jit(solution)/shard_map/all_to_all | solution.py:14
  180.4 27.2 %collective-permute-start.1 = (bf16[3,352,1024]{2,1,0:T(8,128)(2,1)}, bf16[3,352,1024]{2,1,0:T(8,128)(2,1)S(1)}, u32[]{:S(2)}, u32[]{:S(2)}) collective-permute-start(bf16[3,352,1024]{2,1,0:T(8,128)(2,1)} %bitcast.59), channel_id=1, source_target_pairs={{0,1},{1,0},{2,3},{3,2},{4,5},{5,4},{6,7},{7,6},{8,9},{9,8},{10,11... | collective-permute-start | bytes 6488072 | tf_op jit(solution)/shard_map/ppermute | solution.py:22
  200.8 25.5 %all-to-all-start.6 = ((bf16[16,48,1024]{2,1,0:T(8,128)(2,1)}), bf16[16,48,1024]{2,1,0:T(8,128)(2,1)}, u32[]{:S(2)}, u32[]{:S(2)}) async-start(bf16[16,48,1024]{2,1,0:T(8,128)(2,1)} %broadcast_in_dim.18), calls=%async_computation.6 | async-start | bytes 3145728 | tf_op jit(solution)/shard_map/all_to_all | solution.py:14
  207.9 2.0 copy-start.3
  279.3 29.2 %all-to-all-start.10 = ((bf16[16,192,256]{2,1,0:T(8,128)(2,1)}), bf16[16,192,256]{2,1,0:T(8,128)(2,1)S(1)}, u32[]{:S(2)}, u32[]{:S(2)}) async-start(bf16[16,192,256]{2,1,0:T(8,128)(2,1)} %bitcast.84), calls=%async_computation.10 | async-start | bytes 3145728 | tf_op jit(solution)/shard_map/all_to_all | solution.py:14
  308.6 57.3 %copy-start.1 = (bf16[1536,256]{1,0:T(8,128)(2,1)S(1)}, bf16[1536,256]{1,0:T(8,128)(2,1)}, u32[]{:S(2)}) copy-start(bf16[1536,256]{1,0:T(8,128)(2,1)} %param.6) | copy-start | bytes 2359300
  353.0 11.7 %collective-permute-start.2 = (bf16[768,256]{1,0:T(8,128)(2,1)S(1)}, bf16[768,256]{1,0:T(8,128)(2,1)S(1)}, u32[]{:S(2)}, u32[]{:S(2)}) collective-permute-start(bf16[768,256]{1,0:T(8,128)(2,1)S(1)} %bitcast.97), channel_id=1, source_target_pairs={{0,1},{1,0},{2,3},{3,2},{4,5},{5,4},{6,7},{7,6},{8,9},{9,8},{10,11... | collective-permute-start | bytes 1179656 | tf_op jit(solution)/shard_map/ppermute | solution.py:22
where the time goes:
time: 367 us; the launch traced here: 366 us
  blocking collectives  177 us (48%)
  waiting for transfers between devices  76.9 us (21%)
  starting transfers between devices  52.9 us (14%)
  local copies, waits for them, and re-layouts  31.9 us (9%)
  matrix products  18.1 us (5%)
  other arithmetic  8.87 us (2%)
    all_to_all x6, blocking collectives, exchange(): return lax.all_to_all(parts, axes, 0, 0, tiled=True)  119 us
    all_to_all x6, waiting for transfers between devices, exchange(): return lax.all_to_all(parts, axes, 0, 0, tiled=True)  75.6 us
    all_to_all x6, starting transfers between devices, exchange(): return lax.all_to_all(parts, axes, 0, 0, tiled=True)  32.1 us
    psum x1, blocking collectives, per_device(): lax.psum(jnp.stack((mixed.sum(axis=1), (mixed * mixed).sum(axis=1))), ('z...  31.9 us
    ppermute x3, starting transfers between devices, swap_core(): return lax.ppermute(block, 'c', [(0, 1), (1, 0)])  20.8 us
    all_gather x1, blocking collectives, per_device(): affine = lax.all_gather(affine, 'x', axis=1, tiled=True)  18.8 us
    dot_general x2, matrix products, dot_nt(): lax.dot_general(a, b, (((1,), (1,)), ((), ())), preferred_element_type=F32)  9.85 us
  transfers between devices with their start and end apart: 9, of which 6 were waited for; matrix products, arithmetic and copies ran while one was open for 6% of the time, Pallas kernels for 0%

commit v1 on v0

--- a/solution.py
+++ b/solution.py
@@ -80,7 +80,9 @@
     branch = exchange(parts, ("x", "y")).astype(F32).sum(axis=0)
     own = lax.dynamic_slice(stream, (y * quarter, x * 256), (quarter, 256))
     mixed = RESIDUAL * own.astype(F32) + branch
-    stats = lax.psum(jnp.stack((mixed.sum(axis=1), (mixed * mixed).sum(axis=1))), ("z", "x"))
+    stats = lax.psum(
+        lax.psum(jnp.stack((mixed.sum(axis=1), (mixed * mixed).sum(axis=1))), "x"), "z"
+    )
     out = normed(mixed, stats[0], stats[1], norm_gain[1], norm_shift[1])
     ours = share(out, "y", 4).reshape(half, 256)
     theirs = swap_core(ours)

time: 367 us -> 348 us (0.948)
  blocking collectives: 177 us -> 160 us
    psum x1 -> x2, blocking collectives: 31.9 us -> 15.7 us  [the longest x1 8.84 us: per_device(): lax.psum(jnp.stack((mixed.sum(axis=1), (mixed * mixed).sum(axis=1))), 'x')]
  transfers between devices with their start and end apart: 9 -> 9, of which waited for: 6 -> 6; matrix products, arithmetic and copies ran while one was open for 6% -> 7% of each run, Pallas kernels for 0% -> 0%
where the time goes in v1:
time: 348 us; the launch traced here: 346 us
  blocking collectives  160 us (46%)
  waiting for transfers between devices  76.8 us (22%)
  starting transfers between devices  49.9 us (14%)
  local copies, waits for them, and re-layouts  31.9 us (9%)
  matrix products  18.1 us (5%)
  other arithmetic  8.87 us (3%)
    all_to_all x6, blocking collectives, exchange(): return lax.all_to_all(parts, axes, 0, 0, tiled=True)  119 us
    all_to_all x6, waiting for transfers between devices, exchange(): return lax.all_to_all(parts, axes, 0, 0, tiled=True)  75.4 us
    all_to_all x6, starting transfers between devices, exchange(): return lax.all_to_all(parts, axes, 0, 0, tiled=True)  32 us
    all_gather x1, blocking collectives, per_device(): affine = lax.all_gather(affine, 'x', axis=1, tiled=True)  18.8 us
    ppermute x3, starting transfers between devices, swap_core(): return lax.ppermute(block, 'c', [(0, 1), (1, 0)])  17.9 us
    dot_general x2, matrix products, dot_nt(): lax.dot_general(a, b, (((1,), (1,)), ((), ())), preferred_element_type=F32)  9.85 us
    psum x1, blocking collectives, per_device(): lax.psum(jnp.stack((mixed.sum(axis=1), (mixed * mixed).sum(axis=1))), 'x')  8.84 us
    unnamed x24, local copies, waits for them, and re-layouts  7.21 us
  transfers between devices with their start and end apart: 9, of which 6 were waited for; matrix products, arithmetic and copies ran while one was open for 7% of the time, Pallas kernels for 0%

profile of v1, /device:TPU:1, one launch (start us, length us, event | category | flops | bytes accessed | tf_op | source)
XLA Modules:
  0.0 346.3 jit_solution(16271070420660406616)
XLA Ops:
  0.0 2.4 fusion.6
  2.6 2.3 fusion.7
  5.2 2.3 fusion.8
  7.9 30.5 %all_to_all.60 = bf16[4,3,352,256]{3,2,1,0:T(8,128)(2,1)S(1)} all-to-all(bf16[4,3,352,256]{3,2,1,0:T(8,128)(2,1)S(1)} %copy.30), channel_id=1, replica_groups=mesh['z'=4,'x'=4,'y'=4,'c'=2] {'x'}, dimensions={0} | all-to-all | bytes 4325376 | tf_op jit(solution)/shard_map/all_to_all | solution.py:14
  38.7 2.2 collective-permute-start
  40.9 10.2 %all_to_all.61 = bf16[4,192,256]{2,1,0:T(8,128)(2,1)S(1)} all-to-all(bf16[4,192,256]{2,1,0:T(8,128)(2,1)S(1)} %broadcast_in_dim.14), channel_id=1, replica_groups=mesh['z'=4,'x'=4,'y'=4,'c'=2] {'x'}, dimensions={0} | all-to-all | bytes 786432 | tf_op jit(solution)/shard_map/all_to_all | solution.py:14
  52.6 4.3 %all-to-all-start.1 = ((bf16[4,192,1024]{2,1,0:T(8,128)(2,1)}), bf16[4,192,1024]{2,1,0:T(8,128)(2,1)}, u32[]{:S(2)}, u32[]{:S(2)}) async-start(bf16[4,192,1024]{2,1,0:T(8,128)(2,1)} %broadcast_in_dim.16), calls=%async_computation.1 | async-start | bytes 3145728 | tf_op jit(solution)/shard_map/all_to_all | solution.py:14
  62.9 13.6 %all-to-all-done.1 = bf16[4,192,1024]{2,1,0:T(8,128)(2,1)} async-done(((bf16[4,192,1024]{2,1,0:T(8,128)(2,1)}), bf16[4,192,1024]{2,1,0:T(8,128)(2,1)}, u32[]{:S(2)}, u32[]{:S(2)}) %all-to-all-start.1) | async-done | bytes 1572896 | tf_op jit(solution)/shard_map/all_to_all | solution.py:14
  76.5 4.9 %convolution_convert_fusion.1 = bf16[768,1408]{1,0:T(8,128)(2,1)S(1)} fusion(bf16[768,1024]{1,0:T(8,128)(2,1)} %bitcast.1, bf16[1408,1024]{1,0:T(8,128)(2,1)} %bitcast.85), kind=kOutput, calls=%fused_computation.3 | convolution fusion | flops 2215673856 | bytes 6619136 | tf_op jit(solution)/shard_map/dot_general | solution.py:26
  81.4 29.2 %all_to_all.62 = bf16[4,192,1408]{2,1,0:T(8,128)(2,1)S(1)} all-to-all(bf16[4,192,1408]{2,1,0:T(8,128)(2,1)S(1)} %bitcast.93), channel_id=1, replica_groups=mesh['z'=4,'x'=4,'y'=4,'c'=2] {'z'}, dimensions={0} | all-to-all | bytes 4325376 | tf_op jit(solution)/shard_map/all_to_all | solution.py:14
  112.3 4.4 %all-to-all-start.4 = ((bf16[4,192,704]{2,1,0:T(8,128)(2,1)}), bf16[4,192,704]{2,1,0:T(8,128)(2,1)}, u32[]{:S(2)}, u32[]{:S(2)}) async-start(bf16[4,192,704]{2,1,0:T(8,128)(2,1)} %broadcast_in_dim.17), calls=%async_computation.4 | async-start | bytes 2359296 | tf_op jit(solution)/shard_map/all_to_all | solution.py:14
  119.1 10.4 %all-to-all-done.4 = bf16[4,192,704]{2,1,0:T(8,128)(2,1)} async-done(((bf16[4,192,704]{2,1,0:T(8,128)(2,1)}), bf16[4,192,704]{2,1,0:T(8,128)(2,1)}, u32[]{:S(2)}, u32[]{:S(2)}) %all-to-all-start.4) | async-done | bytes 1081376 | tf_op jit(solution)/shard_map/all_to_all | solution.py:14
  129.4 3.6 %all-to-all-start.7 = ((bf16[4,3,352,256]{3,2,1,0:T(8,128)(2,1)}), bf16[4,3,352,256]{3,2,1,0:T(8,128)(2,1)S(1)}, u32[]{:S(2)}, u32[]{:S(2)}) async-start(bf16[4,3,352,256]{3,2,1,0:T(8,128)(2,1)} %copy.34), calls=%async_computation.7 | async-start | bytes 4325376 | tf_op jit(solution)/shard_map/all_to_all | solution.py:14
  133.1 4.3 %convolution_convert_fusion.3 = bf16[768,1024]{1,0:T(8,128)(2,1)} fusion(bf16[768,704]{1,0:T(8,128)(2,1)} %bitcast.13, bf16[3,704,1024]{2,1,0:T(8,128)(2,1)} %copy-done.2), kind=kOutput, calls=%fused_computation.9 | convolution fusion | flops 1108082688 | bytes 4194304 | tf_op jit(solution)/shard_map/dot_general | solution.py:69
  137.4 18.0 %all-to-all-done.7 = bf16[4,3,352,256]{3,2,1,0:T(8,128)(2,1)S(1)} async-done(((bf16[4,3,352,256]{3,2,1,0:T(8,128)(2,1)}), bf16[4,3,352,256]{3,2,1,0:T(8,128)(2,1)S(1)}, u32[]{:S(2)}, u32[]{:S(2)}) %all-to-all-start.7) | async-done | bytes 2162720 | tf_op jit(solution)/shard_map/all_to_all | solution.py:14
  155.3 4.4 %all-to-all-start.5 = ((bf16[16,48,1024]{2,1,0:T(8,128)(2,1)}), bf16[16,48,1024]{2,1,0:T(8,128)(2,1)}, u32[]{:S(2)}, u32[]{:S(2)}) async-start(bf16[16,48,1024]{2,1,0:T(8,128)(2,1)} %bitcast.95), calls=%async_computation.5 | async-start | bytes 3145728 | tf_op jit(solution)/shard_map/all_to_all | solution.py:14
  159.8 18.8 %all_gather.3 = f32[2,1024]{1,0:T(2,128)S(1)} all-gather(f32[2,256]{1,0:T(2,128)S(1)} %pad_maximum_fusion), channel_id=1, replica_groups=mesh['z'=4,'x'=4,'y'=4,'c'=2] {'x'}, dimensions={1}, use_global_device_ids=true | all-gather | bytes 10240 | tf_op jit(solution)/shard_map/all_gather | solution.py:65
  180.3 8.3 %collective-permute-start.1 = (bf16[3,352,1024]{2,1,0:T(8,128)(2,1)}, bf16[3,352,1024]{2,1,0:T(8,128)(2,1)S(1)}, u32[]{:S(2)}, u32[]{:S(2)}) collective-permute-start(bf16[3,352,1024]{2,1,0:T(8,128)(2,1)} %bitcast.59), channel_id=1, source_target_pairs={{0,1},{1,0},{2,3},{3,2},{4,5},{5,4},{6,7},{7,6},{8,9},{9,8},{10,11... | collective-permute-start | bytes 6488072 | tf_op jit(solution)/shard_map/ppermute | solution.py:22
  191.4 6.9 %psum.21 = f32[2,48]{1,0:T(2,128)S(1)} all-reduce(f32[2,48]{1,0:T(2,128)S(1)} %pad_maximum_fusion.2), channel_id=1, replica_groups=mesh['z'=4,'x'=4,'y'=4,'c'=2] {'z'}, use_global_device_ids=true, to_apply=%region_4.5 | all-reduce | flops 96 | bytes 768 | tf_op jit(solution)/shard_map/psum | solution.py:74
  200.7 5.1 %all-to-all-start.6 = ((bf16[16,48,1024]{2,1,0:T(8,128)(2,1)}), bf16[16,48,1024]{2,1,0:T(8,128)(2,1)}, u32[]{:S(2)}, u32[]{:S(2)}) async-start(bf16[16,48,1024]{2,1,0:T(8,128)(2,1)} %broadcast_in_dim.18), calls=%async_computation.6 | async-start | bytes 3145728 | tf_op jit(solution)/shard_map/all_to_all | solution.py:14
  211.7 14.5 %all-to-all-done.6 = bf16[16,48,1024]{2,1,0:T(8,128)(2,1)} async-done(((bf16[16,48,1024]{2,1,0:T(8,128)(2,1)}), bf16[16,48,1024]{2,1,0:T(8,128)(2,1)}, u32[]{:S(2)}, u32[]{:S(2)}) %all-to-all-start.6) | async-done | bytes 1572896 | tf_op jit(solution)/shard_map/all_to_all | solution.py:14
  226.2 4.9 %convolution_convert_fusion = bf16[768,1408]{1,0:T(8,128)(2,1)S(1)} fusion(bf16[768,1024]{1,0:T(8,128)(2,1)} %bitcast.22, bf16[1408,1024]{1,0:T(8,128)(2,1)} %bitcast.86), kind=kOutput, calls=%fused_computation.2 | convolution fusion | flops 2215673856 | bytes 6619136 | tf_op jit(solution)/shard_map/dot_general | solution.py:26
  231.1 25.4 %all_to_all.63 = bf16[4,192,1408]{2,1,0:T(8,128)(2,1)S(1)} all-to-all(bf16[4,192,1408]{2,1,0:T(8,128)(2,1)S(1)} %bitcast.94), channel_id=1, replica_groups=mesh['z'=4,'x'=4,'y'=4,'c'=2] {'z'}, dimensions={0} | all-to-all | bytes 4325376 | tf_op jit(solution)/shard_map/all_to_all | solution.py:14
  257.2 13.7 %all_to_all.64 = bf16[4,192,704]{2,1,0:T(8,128)(2,1)S(1)} all-to-all(bf16[4,192,704]{2,1,0:T(8,128)(2,1)S(1)} %broadcast_in_dim.19), channel_id=1, replica_groups=mesh['z'=4,'x'=4,'y'=4,'c'=2] {'z'}, dimensions={0} | all-to-all | bytes 2162688 | tf_op jit(solution)/shard_map/all_to_all | solution.py:14
  271.0 3.9 %convolution_convert_fusion.2 = bf16[768,1024]{1,0:T(8,128)(2,1)} fusion(bf16[768,704]{1,0:T(8,128)(2,1)S(1)} %bitcast.100, bf16[3,704,1024]{2,1,0:T(8,128)(2,1)} %copy-done.3), kind=kOutput, calls=%fused_computation.8 | convolution fusion | flops 1108082688 | bytes 4096000 | tf_op jit(solution)/shard_map/dot_general | solution.py:78
  274.9 2.9 reshape.113
  279.2 10.2 %all-to-all-start.10 = ((bf16[16,192,256]{2,1,0:T(8,128)(2,1)}), bf16[16,192,256]{2,1,0:T(8,128)(2,1)S(1)}, u32[]{:S(2)}, u32[]{:S(2)}) async-start(bf16[16,192,256]{2,1,0:T(8,128)(2,1)} %bitcast.84), calls=%async_computation.10 | async-start | bytes 3145728 | tf_op jit(solution)/shard_map/all_to_all | solution.py:14
  289.4 19.0 %all-to-all-done.10 = bf16[16,192,256]{2,1,0:T(8,128)(2,1)S(1)} async-done(((bf16[16,192,256]{2,1,0:T(8,128)(2,1)}), bf16[16,192,256]{2,1,0:T(8,128)(2,1)S(1)}, u32[]{:S(2)}, u32[]{:S(2)}) %all-to-all-start.10) | async-done | bytes 1572896 | tf_op jit(solution)/shard_map/all_to_all | solution.py:14
  309.8 8.8 %psum.22 = f32[2,192]{1,0:T(2,128)S(1)} all-reduce(f32[2,192]{1,0:T(2,128)S(1)} %pad_maximum_fusion.1), channel_id=1, replica_groups=mesh['z'=4,'x'=4,'y'=4,'c'=2] {'x'}, use_global_device_ids=true, to_apply=%region_9.10 | all-reduce | flops 384 | bytes 3072 | tf_op jit(solution)/shard_map/psum | solution.py:84
  318.6 6.9 %psum.23 = f32[2,192]{1,0:T(2,128)S(1)} all-reduce(f32[2,192]{1,0:T(2,128)S(1)} %psum.22), channel_id=1, replica_groups=mesh['z'=4,'x'=4,'y'=4,'c'=2] {'z'}, use_global_device_ids=true, to_apply=%region_10.11 | all-reduce | flops 384 | bytes 3072 | tf_op jit(solution)/shard_map/psum | solution.py:83
  326.5 9.8 %all_to_all.65 = bf16[4,192,256]{2,1,0:T(8,128)(2,1)S(1)} all-to-all(bf16[4,192,256]{2,1,0:T(8,128)(2,1)S(1)} %broadcast_in_dim.20), channel_id=1, replica_groups=mesh['z'=4,'x'=4,'y'=4,'c'=2] {'y'}, dimensions={0} | all-to-all | bytes 786432 | tf_op jit(solution)/shard_map/all_to_all | solution.py:14
  336.4 7.4 %collective-permute-start.2 = (bf16[768,256]{1,0:T(8,128)(2,1)S(1)}, bf16[768,256]{1,0:T(8,128)(2,1)S(1)}, u32[]{:S(2)}, u32[]{:S(2)}) collective-permute-start(bf16[768,256]{1,0:T(8,128)(2,1)S(1)} %bitcast.97), channel_id=1, source_target_pairs={{0,1},{1,0},{2,3},{3,2},{4,5},{5,4},{6,7},{7,6},{8,9},{9,8},{10,11... | collective-permute-start | bytes 1179656 | tf_op jit(solution)/shard_map/ppermute | solution.py:22
  (67 shorter events, 32.3 us)
Async XLA Ops:
  0.0 40.9 %copy-start = (bf16[1536,256]{1,0:T(8,128)(2,1)S(1)}, bf16[1536,256]{1,0:T(8,128)(2,1)}, u32[]{:S(2)}) copy-start(bf16[1536,256]{1,0:T(8,128)(2,1)} %param.6) | copy-start | bytes 2359300
  38.7 18.5 %collective-permute-start = (bf16[3,352,1024]{2,1,0:T(8,128)(2,1)S(1)}, bf16[3,352,1024]{2,1,0:T(8,128)(2,1)}, u32[]{:S(2)}, u32[]{:S(2)}) collective-permute-start(bf16[3,352,1024]{2,1,0:T(8,128)(2,1)S(1)} %bitcast.81), channel_id=1, source_target_pairs={{0,1},{1,0},{2,3},{3,2},{4,5},{5,4},{6,7},{7,6},{8,9},{9,8},{10,11... | collective-permute-start | bytes 6488072 | tf_op jit(solution)/shard_map/ppermute | solution.py:22
  52.6 23.8 %all-to-all-start.1 = ((bf16[4,192,1024]{2,1,0:T(8,128)(2,1)}), bf16[4,192,1024]{2,1,0:T(8,128)(2,1)}, u32[]{:S(2)}, u32[]{:S(2)}) async-start(bf16[4,192,1024]{2,1,0:T(8,128)(2,1)} %broadcast_in_dim.16), calls=%async_computation.1 | async-start | bytes 3145728 | tf_op jit(solution)/shard_map/all_to_all | solution.py:14
  59.0 2.1 copy-start.2
  111.1 5.6 %copy-start.4 = (bf16[1,256,1408]{2,1,0:T(8,128)(2,1)S(1)}, bf16[1,256,1408]{2,1,0:T(8,128)(2,1)}, u32[]{:S(2)}) copy-start(bf16[1,256,1408]{2,1,0:T(8,128)(2,1)} %get-tuple-element.9) | copy-start | bytes 2162692
  112.3 4.7 %copy-start.5 = (bf16[1,256,1408]{2,1,0:T(8,128)(2,1)S(1)}, bf16[1,256,1408]{2,1,0:T(8,128)(2,1)}, u32[]{:S(2)}) copy-start(bf16[1,256,1408]{2,1,0:T(8,128)(2,1)} %get-tuple-element.11) | copy-start | bytes 2162692
  112.3 5.0 %copy-start.6 = (bf16[1,1408,256]{2,1,0:T(8,128)(2,1)S(1)}, bf16[1,1408,256]{2,1,0:T(8,128)(2,1)}, u32[]{:S(2)}) copy-start(bf16[1,1408,256]{2,1,0:T(8,128)(2,1)} %get-tuple-element.13) | copy-start | bytes 2162692
  112.3 17.1 %all-to-all-start.4 = ((bf16[4,192,704]{2,1,0:T(8,128)(2,1)}), bf16[4,192,704]{2,1,0:T(8,128)(2,1)}, u32[]{:S(2)}, u32[]{:S(2)}) async-start(bf16[4,192,704]{2,1,0:T(8,128)(2,1)} %broadcast_in_dim.17), calls=%async_computation.4 | async-start | bytes 2359296 | tf_op jit(solution)/shard_map/all_to_all | solution.py:14
  129.4 25.9 %all-to-all-start.7 = ((bf16[4,3,352,256]{3,2,1,0:T(8,128)(2,1)}), bf16[4,3,352,256]{3,2,1,0:T(8,128)(2,1)S(1)}, u32[]{:S(2)}, u32[]{:S(2)}) async-start(bf16[4,3,352,256]{3,2,1,0:T(8,128)(2,1)} %copy.34), calls=%async_computation.7 | async-start | bytes 4325376 | tf_op jit(solution)/shard_map/all_to_all | solution.py:14
  137.4 22.4 %copy-start.7 = (f32[2,256]{1,0:T(2,128)S(1)}, f32[2,256]{1,0:T(2,128)}, u32[]{:S(2)}) copy-start(f32[2,256]{1,0:T(2,128)} %param.10) | copy-start | bytes 6148
  137.4 22.4 %copy-start.8 = (f32[2,256]{1,0:T(2,128)S(1)}, f32[2,256]{1,0:T(2,128)}, u32[]{:S(2)}) copy-start(f32[2,256]{1,0:T(2,128)} %param.11) | copy-start | bytes 6148
  155.3 33.2 %all-to-all-start.5 = ((bf16[16,48,1024]{2,1,0:T(8,128)(2,1)}), bf16[16,48,1024]{2,1,0:T(8,128)(2,1)}, u32[]{:S(2)}, u32[]{:S(2)}) async-start(bf16[16,48,1024]{2,1,0:T(8,128)(2,1)} %bitcast.95), calls=%async_computation.5 | async-start | bytes 3145728 | tf_op jit(solution)/shard_map/all_to_all | solution.py:14
  180.3 27.3 %collective-permute-start.1 = (bf16[3,352,1024]{2,1,0:T(8,128)(2,1)}, bf16[3,352,1024]{2,1,0:T(8,128)(2,1)S(1)}, u32[]{:S(2)}, u32[]{:S(2)}) collective-permute-start(bf16[3,352,1024]{2,1,0:T(8,128)(2,1)} %bitcast.59), channel_id=1, source_target_pairs={{0,1},{1,0},{2,3},{3,2},{4,5},{5,4},{6,7},{7,6},{8,9},{9,8},{10,11... | collective-permute-start | bytes 6488072 | tf_op jit(solution)/shard_map/ppermute | solution.py:22
  200.7 25.6 %all-to-all-start.6 = ((bf16[16,48,1024]{2,1,0:T(8,128)(2,1)}), bf16[16,48,1024]{2,1,0:T(8,128)(2,1)}, u32[]{:S(2)}, u32[]{:S(2)}) async-start(bf16[16,48,1024]{2,1,0:T(8,128)(2,1)} %broadcast_in_dim.18), calls=%async_computation.6 | async-start | bytes 3145728 | tf_op jit(solution)/shard_map/all_to_all | solution.py:14
  207.7 2.0 copy-start.3
  279.2 29.2 %all-to-all-start.10 = ((bf16[16,192,256]{2,1,0:T(8,128)(2,1)}), bf16[16,192,256]{2,1,0:T(8,128)(2,1)S(1)}, u32[]{:S(2)}, u32[]{:S(2)}) async-start(bf16[16,192,256]{2,1,0:T(8,128)(2,1)} %bitcast.84), calls=%async_computation.10 | async-start | bytes 3145728 | tf_op jit(solution)/shard_map/all_to_all | solution.py:14
  308.4 37.8 %copy-start.1 = (bf16[1536,256]{1,0:T(8,128)(2,1)S(1)}, bf16[1536,256]{1,0:T(8,128)(2,1)}, u32[]{:S(2)}) copy-start(bf16[1536,256]{1,0:T(8,128)(2,1)} %param.6) | copy-start | bytes 2359300
  336.4 8.7 %collective-permute-start.2 = (bf16[768,256]{1,0:T(8,128)(2,1)S(1)}, bf16[768,256]{1,0:T(8,128)(2,1)S(1)}, u32[]{:S(2)}, u32[]{:S(2)}) collective-permute-start(bf16[768,256]{1,0:T(8,128)(2,1)S(1)} %bitcast.97), channel_id=1, source_target_pairs={{0,1},{1,0},{2,3},{3,2},{4,5},{5,4},{6,7},{7,6},{8,9},{9,8},{10,11... | collective-permute-start | bytes 1179656 | tf_op jit(solution)/shard_map/ppermute | solution.py:22
